TPU v7x, 32 devices: a whole 2x2x4 slice. The times are simulated.
32 devices in a mesh: sp: 16 (over z, y, x), tp: 2 (over core).
Axes of the slice: x: 2, y: 2, z: 4, core: 2. Of those that a mesh axis runs over, the one named last changes fastest.
Arguments:
- residual: bfloat16 [4096, 2048], P('sp'), may hold values from -6 to 6
- queries: bfloat16 [4096, 1024], P('sp', 'tp'), may hold values from -6 to 6
- forget_gate_logits: bfloat16 [4096, 1024], P('sp', 'tp'), may hold values from -5 to 5
- projected_values: bfloat16 [4096, 1024], P('sp', 'tp'), may hold values from -6 to 6
- output_gate_logits: bfloat16 [4096, 1024], P('sp', 'tp'), may hold values from -6 to 6
- lower_bound_margin: float32 [1024], P('tp'), may hold values from 0.00024414062 to 0.08
- extra_forget_logs: float32 [4096, 1024], P('sp', 'tp'), may hold values from -0.7 to 0
- per_head_norm_gain: float32 [128], replicated, may hold values from 0.1 to 1.9
- output_weight: bfloat16 [1024, 2048], P('tp'), may hold values from -0.1875 to 0.1875
- feedforward_norm_gain: float32 [2048], replicated, may hold values from 0.1 to 1.9
- gate_weight: bfloat16 [2048, 5632], P('sp', 'tp'), may hold values from -0.125 to 0.125
- up_weight: bfloat16 [2048, 5632], P('sp', 'tp'), may hold values from -0.125 to 0.125
- down_weight: bfloat16 [5632, 2048], P('tp', 'sp'), may hold values from -0.078125 to 0.078125
Outputs:
- layer_out: bfloat16 [4096, 2048], P('sp')
All inputs are finite; a program needn't handle non-finite values.
Results may differ from a plain program's by a relative error of at most 0.015.
Values may be sent and summed in bfloat16 or wider, within the bound.
A program may use at most 128 MiB of HBM per device.

v0:
```python
import jax
import jax.numpy as jnp
from jax import lax
from jax.sharding import PartitionSpec as P

HD = 128
BLOCK = 64
eps = 1e-06
top_precision = lax.Precision.HIGHEST


def carried_in_2(value, axis, join, neutral):
    place = lax.axis_index(axis)
    gathered = jax.tree.map(
        lambda a, kind: lax.all_gather(a.astype(kind), axis), value, (jnp.bfloat16, jnp.bfloat16)
    )
    state = jax.tree.map(lambda a, e: jnp.zeros_like(a) + jnp.asarray(e, a.dtype), value, neutral)

    def one(turn, state):
        return join(
            state,
            jax.tree.map(
                lambda a, own: lax.dynamic_index_in_dim(a, turn, 0, False).astype(own.dtype),
                gathered,
                value,
            ),
        )

    return lax.fori_loop(0, place, one, state)


def block_update(carried_in, inputs):
    recurrent_state, offset = carried_in
    queries, state_increment, value_rows, retain_log_factor = inputs
    running_state = jnp.cumsum(retain_log_factor, axis=1)
    causal = jnp.tril(
        jnp.ones((retain_log_factor.shape[1], retain_log_factor.shape[1]), dtype=bool)
    )
    carried_over_state = jnp.einsum(
        "uqw,uwa->uqa", queries * jnp.exp(running_state), recurrent_state, precision=top_precision
    )
    spread = running_state[:, :, None, :] - running_state[:, None, :, :]
    weights = jnp.exp(jnp.where(causal[None, :, :, None], spread, -jnp.inf))
    scores = jnp.einsum(
        "htk,htsk,hsk->hts", queries, weights, state_increment, precision=top_precision
    )
    output_rows = carried_over_state + jnp.einsum(
        "hts,hsv->htv", scores, value_rows, precision=top_precision
    )
    final_state = running_state[:, -1:, :]
    updated_state = jnp.exp(final_state[:, 0, :])[:, :, None] * recurrent_state + jnp.einsum(
        "erb,erc->ebc",
        state_increment * jnp.exp(final_state - running_state),
        value_rows,
        precision=top_precision,
    )
    rescaled_state = queries * jnp.exp(running_state + offset[:, None, :])
    return ((updated_state, offset + final_state[:, 0, :]), (output_rows, rescaled_state))


def join_states(earlier, later):
    earlier_sum, earlier_memory = earlier
    later_sum, later_memory = later
    return (earlier_sum + later_sum, jnp.exp(later_sum)[:, :, None] * earlier_memory + later_memory)


def local(
    residual,
    queries,
    forget_gate_logits,
    projected_values,
    output_gate_logits,
    lower_bound_margin,
    extra_forget_logs,
    per_head_norm_gain,
    output_weight,
    feedforward_norm_gain,
    gate_weight,
    up_weight,
    down_weight,
):
    length = queries.shape[0]
    head_count = queries.shape[1] // HD
    state_increment = lower_bound_margin * jax.nn.sigmoid(-forget_gate_logits.astype(jnp.float32))
    retain_log_factor = jnp.log1p(-state_increment) + extra_forget_logs

    def to_blocks(source):
        return source.reshape(length // BLOCK, BLOCK, head_count, HD).transpose(0, 2, 1, 3)

    initial = (
        jnp.zeros((head_count, HD, HD), jnp.float32),
        jnp.zeros((head_count, HD), jnp.float32),
    )
    block_inputs = (
        to_blocks(queries.astype(jnp.float32)),
        to_blocks(state_increment),
        to_blocks(projected_values.astype(jnp.float32)),
        to_blocks(retain_log_factor),
    )
    (recurrent_state, decay_sum), (output_rows, rescaled_state) = lax.scan(
        block_update, initial, block_inputs
    )
    identity = (jnp.zeros_like(decay_sum), jnp.zeros_like(recurrent_state))
    incoming_state = carried_in_2((decay_sum, recurrent_state), "sp", join_states, identity)[1]
    output_rows = output_rows + jnp.einsum(
        "sjey,jyx->sjex", rescaled_state, incoming_state, precision=top_precision
    )
    mixed = output_rows.transpose(0, 2, 1, 3).reshape(length, head_count, HD)
    normed_heads = (
        mixed
        * lax.rsqrt(jnp.mean(mixed * mixed, axis=-1, keepdims=True) + eps)
        * per_head_norm_gain
    )
    gating = jax.nn.silu(output_gate_logits.astype(jnp.float32)).reshape(length, head_count, HD)
    gated = (normed_heads * gating).reshape(length, head_count * HD).astype(jnp.bfloat16)
    row_count = residual.shape[0] // lax.axis_size("tp")
    own_rows = lax.dynamic_slice_in_dim(residual, lax.axis_index("tp") * row_count, row_count, 0)
    rows_here = gated
    projected = lax.psum_scatter(
        jnp.dot(rows_here, output_weight, preferred_element_type=jnp.float32).astype(jnp.bfloat16),
        "tp",
        scatter_dimension=0,
        tiled=True,
    ).astype(jnp.float32)
    after_mixer = (own_rows.astype(jnp.float32) + projected).astype(jnp.bfloat16)
    widened = after_mixer.astype(jnp.float32)
    normed = (
        widened
        * lax.rsqrt(jnp.mean(widened * widened, axis=-1, keepdims=True) + eps)
        * feedforward_norm_gain
    ).astype(jnp.bfloat16)
    gate_full, up_full = (
        lax.all_gather(gate_weight, "sp", axis=0, tiled=True),
        lax.all_gather(up_weight, "sp", axis=0, tiled=True),
    )
    down_full = lax.all_gather(down_weight, "sp", axis=1, tiled=True)
    row_piece = lax.all_gather(normed, "tp", axis=0, tiled=True)
    gate_part = jnp.dot(row_piece, gate_full, preferred_element_type=jnp.float32)
    up_part = jnp.dot(row_piece, up_full, preferred_element_type=jnp.float32)
    hidden = (jax.nn.silu(gate_part) * up_part).astype(jnp.bfloat16)
    rows_here = hidden
    ffn_sum = lax.psum_scatter(
        jnp.dot(rows_here, down_full, preferred_element_type=jnp.float32).astype(jnp.bfloat16),
        "tp",
        scatter_dimension=0,
        tiled=True,
    ).astype(jnp.float32)
    finished = (after_mixer.astype(jnp.float32) + 0.5 * ffn_sum).astype(jnp.bfloat16)
    return lax.all_gather(finished, "tp", axis=0, tiled=True)


def solution(mesh):
    return jax.shard_map(
        local,
        mesh=mesh,
        in_specs=(
            P("sp", None),
            P("sp", "tp"),
            P("sp", "tp"),
            P("sp", "tp"),
            P("sp", "tp"),
            P("tp"),
            P("sp", "tp"),
            P(),
            P("tp", None),
            P(),
            P("sp", "tp"),
            P("sp", "tp"),
            P("tp", "sp"),
        ),
        out_specs=P("sp", None),
        check_vma=False,
    )
```

profile of v0, /device:TPU:0, one launch (start us, length us, event | category | flops | bytes accessed | tf_op | source)
XLA Modules:
  0.0 711.4 jit_solution(5645837955671285264)
XLA Ops:
  6.5 2.4 divide_multiply_fusion
  11.1 1.9 reshape.91
  13.0 1.9 reshape.92
  15.0 75.4 %while.30 = (s32[]{:T(128)}, f32[4,128,128]{2,1,0:T(8,128)S(1)}, f32[4,128]{1,0:T(4,128)S(1)}, f32[4,4,64,128]{3,2,0,1:T(8,128)}, f32[4,4,64,128]{3,2,0,1:T(8,12...) while((s32[]{:T(128)}, f32[4,128,128]{2,1,0:T(8,128)S(1)}, ...), condition=%wide.region_2.3_spmd.clone, body=%wide.region_0.2_spmd.clone.sunk | while | flops 159814656 | bytes 5010573 | solution.py:100
  17.1 14.1 %fusion.72 = f32[4,64,1,64]{3,2,1,0:T(1,128)S(1)} fusion(f32[4,64,128,1]{2,3,1,0:T(1,128)S(1)} %bitcast.133, f32[4,64,128]{2,1,0:T(8,128)S(1)} %bitcast.134, f32[4,64,128]{2,1,0:T(8,128)S(1)} %reduce_window_sum.16, pred[64,64]{1,0:T(8,128)(4,1)S(1)} %iota_compare_fusion.2), kind=kOutput, calls=%fused_computation.2.clone.1 | convolution fusion | flops 31457280 | bytes 462848 | tf_op jit(solution)/shard_map/while/body/eval_jaxpr/htk,htsk,hsk->hts/dot_general | solution.py:44
  35.9 14.1 %fusion.72 = f32[4,64,1,64]{3,2,1,0:T(1,128)S(1)} fusion(f32[4,64,128,1]{2,3,1,0:T(1,128)S(1)} %bitcast.133, f32[4,64,128]{2,1,0:T(8,128)S(1)} %bitcast.134, f32[4,64,128]{2,1,0:T(8,128)S(1)} %reduce_window_sum.16, pred[64,64]{1,0:T(8,128)(4,1)S(1)} %iota_compare_fusion.2), kind=kOutput, calls=%fused_computation.2.clone.1 | convolution fusion | flops 31457280 | bytes 462848 | tf_op jit(solution)/shard_map/while/body/eval_jaxpr/htk,htsk,hsk->hts/dot_general | solution.py:44
  54.8 14.1 %fusion.72 = f32[4,64,1,64]{3,2,1,0:T(1,128)S(1)} fusion(f32[4,64,128,1]{2,3,1,0:T(1,128)S(1)} %bitcast.133, f32[4,64,128]{2,1,0:T(8,128)S(1)} %bitcast.134, f32[4,64,128]{2,1,0:T(8,128)S(1)} %reduce_window_sum.16, pred[64,64]{1,0:T(8,128)(4,1)S(1)} %iota_compare_fusion.2), kind=kOutput, calls=%fused_computation.2.clone.1 | convolution fusion | flops 31457280 | bytes 462848 | tf_op jit(solution)/shard_map/while/body/eval_jaxpr/htk,htsk,hsk->hts/dot_general | solution.py:44
  73.6 14.1 %fusion.72 = f32[4,64,1,64]{3,2,1,0:T(1,128)S(1)} fusion(f32[4,64,128,1]{2,3,1,0:T(1,128)S(1)} %bitcast.133, f32[4,64,128]{2,1,0:T(8,128)S(1)} %bitcast.134, f32[4,64,128]{2,1,0:T(8,128)S(1)} %reduce_window_sum.16, pred[64,64]{1,0:T(8,128)(4,1)S(1)} %iota_compare_fusion.2), kind=kOutput, calls=%fused_computation.2.clone.1 | convolution fusion | flops 31457280 | bytes 462848 | tf_op jit(solution)/shard_map/while/body/eval_jaxpr/htk,htsk,hsk->hts/dot_general | solution.py:44
  91.1 42.6 %all-gather.2 = bf16[16,4,128]{2,1,0:T(4,128)(2,1)S(1)} all-gather(bf16[1,4,128]{2,1,0:T(4,128)(2,1)S(1)} %convert_bitcast_fusion), channel_id=2, replica_groups=mesh['sp'=16,'tp'=2] {'sp'}, dimensions={0}, use_global_device_ids=true | all-gather | bytes 17408 | tf_op jit(solution)/shard_map/all_gather | solution.py:15
  133.7 20.7 %all-gather.20.cloned.1.call-done = bf16[64,128,128]{2,1,0:T(8,128)(2,1)} async-done(((bf16[4,128,128]{2,1,0:T(8,128)(2,1)}), bf16[64,128,128]{2,1,0:T(8,128)(2,1)}) %all-gather.20.cloned.1.call-update) | async-done | bytes 2097168 | tf_op jit(solution)/shard_map/all_gather | solution.py:15
  154.4 1.8 multiply_reduce_fusion
  157.0 2.7 convolution_convert_fusion.1
  159.8 24.2 %reduce-scatter.3.cloned.1.call-done = bf16[128,2048]{1,0:T(8,128)(2,1)} async-done(((bf16[256,2048]{1,0:T(8,128)(2,1)}), bf16[128,2048]{1,0:T(8,128)(2,1)}) %reduce-scatter.3.cloned.1.call-update) | async-done | bytes 524304 | tf_op jit(solution)/shard_map/reduce_scatter | solution.py:119
  184.0 1.5 fusion.30
  188.3 8.6 %all-gather.10.cloned.1.call-done = bf16[256,2048]{1,0:T(8,128)(2,1)} async-done(((bf16[128,2048]{1,0:T(8,128)(2,1)}), bf16[256,2048]{1,0:T(8,128)(2,1)}) %all-gather.10.cloned.1.call-update) | async-done | bytes 1048592 | tf_op jit(solution)/shard_map/all_gather | solution.py:137
  196.9 145.2 %all-gather.12.cloned.1.call-done = bf16[2048,2816]{1,0:T(8,128)(2,1)} async-done(((bf16[128,2816]{1,0:T(8,128)(2,1)}), bf16[2048,2816]{1,0:T(8,128)(2,1)}) %all-gather.12.cloned.1.call-update) | async-done | bytes 11534352 | tf_op jit(solution)/shard_map/all_gather | solution.py:133
  342.2 9.4 %fusion.47 = f32[256,2816]{1,0:T(8,128)} fusion(bf16[256,2048]{1,0:T(8,128)(2,1)} %all-gather.10.cloned.1.call-done, bf16[2048,2816]{1,0:T(8,128)(2,1)} %all-gather.12.cloned.1.call-done), kind=kOutput, calls=%fused_computation.80 | convolution fusion | flops 2952790016 | bytes 15466496 | tf_op jit(solution)/shard_map/dot_general | solution.py:138
  351.6 132.9 %all-gather.14.cloned.1.call-done = bf16[2048,2816]{1,0:T(8,128)(2,1)} async-done(((bf16[128,2816]{1,0:T(8,128)(2,1)}), bf16[2048,2816]{1,0:T(8,128)(2,1)}) %all-gather.14.cloned.1.call-update) | async-done | bytes 11534352 | tf_op jit(solution)/shard_map/all_gather | solution.py:134
  484.4 182.8 %all-gather.16.cloned.1.call-done = bf16[2816,2048]{1,0:T(8,128)(2,1)} async-done(((bf16[2816,128]{1,0:T(8,128)(2,1)}), bf16[2816,2048]{1,0:T(8,128)(2,1)}) %all-gather.16.cloned.1.call-update) | async-done | bytes 11534352 | tf_op jit(solution)/shard_map/all_gather | solution.py:136
  667.2 15.8 %convolution_convert_fusion = bf16[256,2048]{1,0:T(8,128)(2,1)} fusion(bf16[2816,2048]{1,0:T(8,128)(2,1)} %all-gather.16.cloned.1.call-done, bf16[256,2048]{1,0:T(8,128)(2,1)} %all-gather.10.cloned.1.call-done, bf16[2048,2816]{1,0:T(8,128)(2,1)} %all-gather.14.cloned.1.call-done, f32[256,2816]{1,0:T(8,128)} %fusion.47), kind=kOutput, calls=%fused_computation.45 | convolution fusion | flops 5910429696 | bytes 28049408 | tf_op jit(solution)/shard_map/dot_general | solution.py:143
  683.1 6.7 reduce-scatter.5.cloned.1.call-done
  689.8 2.0 fusion.33
  691.8 10.4 %all-gather.18.cloned.1.call-done = bf16[256,2048]{1,0:T(8,128)(2,1)} async-done(((bf16[128,2048]{1,0:T(8,128)(2,1)}), bf16[256,2048]{1,0:T(8,128)(2,1)}) %all-gather.18.cloned.1.call-update) | async-done | bytes 1048592 | tf_op jit(solution)/shard_map/all_gather | solution.py:149
  702.2 2.3 copy.110
  (93 shorter events, 25.6 us)
Async XLA Ops:
  6.5 150.5 %copy-start = (bf16[512,2048]{1,0:T(8,128)(2,1)S(1)}, bf16[512,2048]{1,0:T(8,128)(2,1)}, u32[]{:S(2)}) copy-start(bf16[512,2048]{1,0:T(8,128)(2,1)} %param.25) | copy-start | bytes 6291460
  6.5 147.8 %all-gather.20.cloned.1.call-start = ((), (), s32[]{:S(2)}) async-start(), calls=%async_computation.9 | async-start | bytes 2228224 | tf_op jit(solution)/shard_map/all_gather | solution.py:15
  15.0 118.7 %copy-start.3 = (f32[128]{0:T(128)S(1)}, f32[128]{0:T(128)}, u32[]{:S(2)}) copy-start(f32[128]{0:T(128)} %param.24) | copy-start | bytes 1540
  90.4 64.0 %copy-start.1 = (f32[4,4,64,128]{3,2,0,1:T(8,128)S(1)}, f32[4,4,64,128]{3,2,0,1:T(8,128)}, u32[]{:S(2)}) copy-start(f32[4,4,64,128]{3,2,0,1:T(8,128)} %get-tuple-element.99) | copy-start | bytes 1572868
  91.1 93.0 %reduce-scatter.3.cloned.1.call-start = ((), (), s32[]{:S(2)}) async-start(), calls=%async_computation.2 | async-start | bytes 1572864 | tf_op jit(solution)/shard_map/reduce_scatter | solution.py:119
  157.0 28.5 %copy-start.2 = (f32[2048]{0:T(1024)S(1)}, f32[2048]{0:T(1024)}, u32[]{:S(2)}) copy-start(f32[2048]{0:T(1024)} %param.26) | copy-start | bytes 24580
  159.8 37.2 %all-gather.10.cloned.1.call-start = ((), (), s32[]{:S(2)}) async-start(), calls=%async_computation.3 | async-start | bytes 1572864 | tf_op jit(solution)/shard_map/all_gather | solution.py:137
  186.5 155.6 %all-gather.12.cloned.1.call-start = ((), (), s32[]{:S(2)}) async-start(), calls=%async_computation.4 | async-start | bytes 12255232 | tf_op jit(solution)/shard_map/all_gather | solution.py:133
  187.1 297.3 %all-gather.14.cloned.1.call-start = ((), (), s32[]{:S(2)}) async-start(), calls=%async_computation.5 | async-start | bytes 12255232 | tf_op jit(solution)/shard_map/all_gather | solution.py:134
  187.7 479.5 %all-gather.16.cloned.1.call-start = ((), (), s32[]{:S(2)}) async-start(), calls=%async_computation.6 | async-start | bytes 12255232 | tf_op jit(solution)/shard_map/all_gather | solution.py:136
  188.3 501.5 %reduce-scatter.5.cloned.1.call-start = ((), (), s32[]{:S(2)}) async-start(), calls=%async_computation.7 | async-start | bytes 1572864 | tf_op jit(solution)/shard_map/reduce_scatter | solution.py:142
  683.1 19.1 %all-gather.18.cloned.1.call-start = ((), (), s32[]{:S(2)}) async-start(), calls=%async_computation.8 | async-start | bytes 1572864 | tf_op jit(solution)/shard_map/all_gather | solution.py:149
Sparse Core Ops, SparseCore 0:
  91.2 63.1 all-gather.19
  159.9 24.0 reduce-scatter.2
  186.7 10.2 all-gather.9
  199.6 142.5 all-gather.11
  344.8 139.5 all-gather.13
  487.0 180.2 all-gather.15
  683.2 6.5 reduce-scatter.4
  691.9 10.2 all-gather.17
where the time goes:
time: 712 us; the launch traced here: 711 us
  waiting for transfers between devices  533 us (75%)
  matrix products  93.7 us (13%)
  blocking collectives  42.6 us (6%)
  local copies, waits for them, and re-layouts  16.9 us (2%)
  between operations  13.6 us (2%)
  other arithmetic  10.9 us (2%)
    all_gather x1, waiting for transfers between devices, local(): down_full = lax.all_gather(down_weight, 'sp', axis=1, tiled=True)  183 us
    all_gather x1, waiting for transfers between devices, local(): lax.all_gather(gate_weight, 'sp', axis=0, tiled=True)  145 us
    all_gather x1, waiting for transfers between devices, local(): lax.all_gather(up_weight, 'sp', axis=0, tiled=True)  133 us
    dot_general x4, matrix products, block_update(): jnp.einsum('htk,htsk,hsk->hts', queries, weights, state_increment, precis...  56.2 us
    all_gather x1, blocking collectives, carried_in_2(): lax.all_gather(a.astype(kind), axis)  42.6 us
    reduce_scatter x1, waiting for transfers between devices, local(): lax.psum_scatter(jnp.dot(rows_here, output_weight, preferred_element_type...  24.2 us
    all_gather x1, waiting for transfers between devices, carried_in_2(): lax.all_gather(a.astype(kind), axis)  20.7 us
    dot_general x1, matrix products, local(): jnp.dot(rows_here, down_full, preferred_element_type=jnp.float32)  15.8 us
  transfers between devices with their start and end apart: 8, of which 8 were waited for; matrix products, arithmetic and copies ran while one was open for 1% of the time, Pallas kernels for 0%

commit v1 on v0

--- a/solution.py
+++ b/solution.py
@@ -2,6 +2,7 @@
 import jax.numpy as jnp
 from jax import lax
 from jax.sharding import PartitionSpec as P
+from jax.lax import all_gather
 
 HD = 128
 BLOCK = 64
@@ -133,7 +134,7 @@
         lax.all_gather(gate_weight, "sp", axis=0, tiled=True),
         lax.all_gather(up_weight, "sp", axis=0, tiled=True),
     )
-    down_full = lax.all_gather(down_weight, "sp", axis=1, tiled=True)
+    down_full = jnp.concatenate(all_gather(down_weight, axis_name="sp"), 1)
     row_piece = lax.all_gather(normed, "tp", axis=0, tiled=True)
     gate_part = jnp.dot(row_piece, gate_full, preferred_element_type=jnp.float32)
     up_part = jnp.dot(row_piece, up_full, preferred_element_type=jnp.float32)

time: 712 us -> 671 us (0.942)
  waiting for transfers between devices: 533 us -> 476 us
  local copies, waits for them, and re-layouts: 16.9 us -> 32 us
    all_gather x1, waiting for transfers between devices: 183 us -> 142 us  [local(): down_full = jnp.concatenate(all_gather(down_weight, axis_name='sp'), 1)]
    reshape x0 -> x1, local copies, waits for them, and re-layouts: none -> 15.1 us  [local(): down_full = jnp.concatenate(all_gather(down_weight, axis_name='sp'), 1)]
    all_gather x1, waiting for transfers between devices: 8.62 us -> 0.01 us  [local(): row_piece = lax.all_gather(normed, 'tp', axis=0, tiled=True)]
  transfers between devices with their start and end apart: 8 -> 8, of which waited for: 8 -> 7; matrix products, arithmetic and copies ran while one was open for 1% -> 4% of each run, Pallas kernels for 0% -> 0%
where the time goes in v1:
time: 671 us; the launch traced here: 670 us
  waiting for transfers between devices  476 us (71%)
  matrix products  94 us (14%)
  blocking collectives  42.6 us (6%)
  local copies, waits for them, and re-layouts  32 us (5%)
  between operations  13.6 us (2%)
  other arithmetic  10.9 us (2%)
    all_gather x1, waiting for transfers between devices, local(): down_full = jnp.concatenate(all_gather(down_weight, axis_name='sp'), 1)  142 us
    all_gather x1, waiting for transfers between devices, local(): lax.all_gather(gate_weight, 'sp', axis=0, tiled=True)  139 us
    all_gather x1, waiting for transfers between devices, local(): lax.all_gather(up_weight, 'sp', axis=0, tiled=True)  133 us
    dot_general x4, matrix products, block_update(): jnp.einsum('htk,htsk,hsk->hts', queries, weights, state_increment, precis...  56.2 us
    all_gather x1, blocking collectives, carried_in_2(): lax.all_gather(a.astype(kind), axis)  42.6 us
    reduce_scatter x1, waiting for transfers between devices, local(): lax.psum_scatter(jnp.dot(rows_here, output_weight, preferred_element_type...  23.5 us
    all_gather x1, waiting for transfers between devices, carried_in_2(): lax.all_gather(a.astype(kind), axis)  20.7 us
    dot_general x1, matrix products, local(): jnp.dot(rows_here, down_full, preferred_element_type=jnp.float32)  15.9 us
  transfers between devices with their start and end apart: 8, of which 7 were waited for; matrix products, arithmetic and copies ran while one was open for 4% of the time, Pallas kernels for 0%

profile of v1, /device:TPU:0, one launch (start us, length us, event | category | flops | bytes accessed | tf_op | source)
XLA Modules:
  0.0 670.0 jit_solution(2691180283947078787)
XLA Ops:
  6.5 2.4 divide_multiply_fusion
  11.1 1.9 reshape.99
  13.0 1.9 reshape.100
  15.0 75.4 %while.30 = (s32[]{:T(128)}, f32[4,128,128]{2,1,0:T(8,128)S(1)}, f32[4,128]{1,0:T(4,128)S(1)}, f32[4,4,64,128]{3,2,0,1:T(8,128)}, f32[4,4,64,128]{3,2,0,1:T(8,12...) while((s32[]{:T(128)}, f32[4,128,128]{2,1,0:T(8,128)S(1)}, ...), condition=%wide.region_2.3_spmd.clone, body=%wide.region_0.2_spmd.clone.sunk | while | flops 159814656 | bytes 5010573 | solution.py:101
  17.1 14.1 %fusion.72 = f32[4,64,1,64]{3,2,1,0:T(1,128)S(1)} fusion(f32[4,64,128,1]{2,3,1,0:T(1,128)S(1)} %bitcast.139, f32[4,64,128]{2,1,0:T(8,128)S(1)} %bitcast.140, f32[4,64,128]{2,1,0:T(8,128)S(1)} %reduce_window_sum.16, pred[64,64]{1,0:T(8,128)(4,1)S(1)} %iota_compare_fusion.2), kind=kOutput, calls=%fused_computation.2.clone.1 | convolution fusion | flops 31457280 | bytes 462848 | tf_op jit(solution)/shard_map/while/body/eval_jaxpr/htk,htsk,hsk->hts/dot_general | solution.py:45
  35.9 14.1 %fusion.72 = f32[4,64,1,64]{3,2,1,0:T(1,128)S(1)} fusion(f32[4,64,128,1]{2,3,1,0:T(1,128)S(1)} %bitcast.139, f32[4,64,128]{2,1,0:T(8,128)S(1)} %bitcast.140, f32[4,64,128]{2,1,0:T(8,128)S(1)} %reduce_window_sum.16, pred[64,64]{1,0:T(8,128)(4,1)S(1)} %iota_compare_fusion.2), kind=kOutput, calls=%fused_computation.2.clone.1 | convolution fusion | flops 31457280 | bytes 462848 | tf_op jit(solution)/shard_map/while/body/eval_jaxpr/htk,htsk,hsk->hts/dot_general | solution.py:45
  54.8 14.1 %fusion.72 = f32[4,64,1,64]{3,2,1,0:T(1,128)S(1)} fusion(f32[4,64,128,1]{2,3,1,0:T(1,128)S(1)} %bitcast.139, f32[4,64,128]{2,1,0:T(8,128)S(1)} %bitcast.140, f32[4,64,128]{2,1,0:T(8,128)S(1)} %reduce_window_sum.16, pred[64,64]{1,0:T(8,128)(4,1)S(1)} %iota_compare_fusion.2), kind=kOutput, calls=%fused_computation.2.clone.1 | convolution fusion | flops 31457280 | bytes 462848 | tf_op jit(solution)/shard_map/while/body/eval_jaxpr/htk,htsk,hsk->hts/dot_general | solution.py:45
  73.6 14.1 %fusion.72 = f32[4,64,1,64]{3,2,1,0:T(1,128)S(1)} fusion(f32[4,64,128,1]{2,3,1,0:T(1,128)S(1)} %bitcast.139, f32[4,64,128]{2,1,0:T(8,128)S(1)} %bitcast.140, f32[4,64,128]{2,1,0:T(8,128)S(1)} %reduce_window_sum.16, pred[64,64]{1,0:T(8,128)(4,1)S(1)} %iota_compare_fusion.2), kind=kOutput, calls=%fused_computation.2.clone.1 | convolution fusion | flops 31457280 | bytes 462848 | tf_op jit(solution)/shard_map/while/body/eval_jaxpr/htk,htsk,hsk->hts/dot_general | solution.py:45
  91.1 42.6 %all-gather.3 = bf16[16,4,128]{2,1,0:T(4,128)(2,1)S(1)} all-gather(bf16[1,4,128]{2,1,0:T(4,128)(2,1)S(1)} %convert_bitcast_fusion), channel_id=2, replica_groups=mesh['sp'=16,'tp'=2] {'sp'}, dimensions={0}, use_global_device_ids=true | all-gather | bytes 17408 | tf_op jit(solution)/shard_map/all_gather | solution.py:16
  133.7 20.7 %all-gather.19.cloned.1.call-done = bf16[64,128,128]{2,1,0:T(8,128)(2,1)} async-done(((bf16[4,128,128]{2,1,0:T(8,128)(2,1)}), bf16[64,128,128]{2,1,0:T(8,128)(2,1)}) %all-gather.19.cloned.1.call-update) | async-done | bytes 2097168 | tf_op jit(solution)/shard_map/all_gather | solution.py:16
  154.4 1.9 multiply_reduce_fusion
  157.2 2.7 convolution_convert_fusion.1
  160.7 23.5 %reduce-scatter.3.cloned.1.call-done = bf16[128,2048]{1,0:T(8,128)(2,1)} async-done(((bf16[256,2048]{1,0:T(8,128)(2,1)}), bf16[128,2048]{1,0:T(8,128)(2,1)}) %reduce-scatter.3.cloned.1.call-update) | async-done | bytes 524304 | tf_op jit(solution)/shard_map/reduce_scatter | solution.py:120
  184.2 1.5 fusion.30
  187.9 141.7 %all-gather.21.cloned.1.call-done = bf16[45056,128]{1,0:T(8,128)(2,1)} async-done(((bf16[2816,128]{1,0:T(8,128)(2,1)}), bf16[45056,128]{1,0:T(8,128)(2,1)}) %all-gather.21.cloned.1.call-update) | async-done | bytes 11534352 | tf_op jit(solution)/shard_map/all_gather | solution.py:137
  329.6 15.1 %copy.39 = bf16[2816,16,128]{0,2,1:T(8,128)(2,1)} copy(bf16[2816,16,128]{2,0,1:T(8,128)(2,1)} %bitcast.136) | data formatting | bytes 23068672 | tf_op jit(solution)/shard_map/reshape | solution.py:137
  344.7 138.7 %all-gather.13.cloned.1.call-done = bf16[2048,2816]{1,0:T(8,128)(2,1)} async-done(((bf16[128,2816]{1,0:T(8,128)(2,1)}), bf16[2048,2816]{1,0:T(8,128)(2,1)}) %all-gather.13.cloned.1.call-update) | async-done | bytes 11534352 | tf_op jit(solution)/shard_map/all_gather | solution.py:134
  483.5 9.4 %fusion.47 = f32[256,2816]{1,0:T(8,128)} fusion(bf16[256,2048]{1,0:T(8,128)(2,1)} %all-gather.11.cloned.1.call-done, bf16[2048,2816]{1,0:T(8,128)(2,1)} %all-gather.13.cloned.1.call-done), kind=kOutput, calls=%fused_computation.80 | convolution fusion | flops 2952790016 | bytes 15466496 | tf_op jit(solution)/shard_map/dot_general | solution.py:139
  492.9 132.8 %all-gather.15.cloned.1.call-done = bf16[2048,2816]{1,0:T(8,128)(2,1)} async-done(((bf16[128,2816]{1,0:T(8,128)(2,1)}), bf16[2048,2816]{1,0:T(8,128)(2,1)}) %all-gather.15.cloned.1.call-update) | async-done | bytes 11534352 | tf_op jit(solution)/shard_map/all_gather | solution.py:135
  625.7 15.9 %convolution_convert_fusion = bf16[256,2048]{1,0:T(8,128)(2,1)} fusion(bf16[2816,2048]{0,1:T(8,128)(2,1)} %bitcast.137, bf16[256,2048]{1,0:T(8,128)(2,1)} %all-gather.11.cloned.1.call-done, bf16[2048,2816]{1,0:T(8,128)(2,1)} %all-gather.15.cloned.1.call-done, f32[256,2816]{1,0:T(8,128)} %fusion.47), kind=kOutput, calls=%fused_computation.45 | convolution fusion | flops 5910429696 | bytes 28049408 | tf_op jit(solution)/shard_map/dot_general | solution.py:144
  641.8 6.7 reduce-scatter.5.cloned.1.call-done
  648.4 2.0 fusion.33
  650.5 10.4 %all-gather.17.cloned.1.call-done = bf16[256,2048]{1,0:T(8,128)(2,1)} async-done(((bf16[128,2048]{1,0:T(8,128)(2,1)}), bf16[256,2048]{1,0:T(8,128)(2,1)}) %all-gather.17.cloned.1.call-update) | async-done | bytes 1048592 | tf_op jit(solution)/shard_map/all_gather | solution.py:150
  660.9 2.3 copy.119
  (94 shorter events, 25.8 us)
Async XLA Ops:
  6.5 150.6 %copy-start = (bf16[512,2048]{1,0:T(8,128)(2,1)S(1)}, bf16[512,2048]{1,0:T(8,128)(2,1)}, u32[]{:S(2)}) copy-start(bf16[512,2048]{1,0:T(8,128)(2,1)} %param.25) | copy-start | bytes 6291460
  6.5 147.8 %all-gather.19.cloned.1.call-start = ((), (), s32[]{:S(2)}) async-start(), calls=%async_computation.8 | async-start | bytes 2228224 | tf_op jit(solution)/shard_map/all_gather | solution.py:16
  15.0 118.7 %copy-start.3 = (f32[128]{0:T(128)S(1)}, f32[128]{0:T(128)}, u32[]{:S(2)}) copy-start(f32[128]{0:T(128)} %param.24) | copy-start | bytes 1540
  91.0 94.6 %copy-start.2 = (f32[2048]{0:T(1024)S(1)}, f32[2048]{0:T(1024)}, u32[]{:S(2)}) copy-start(f32[2048]{0:T(1024)} %param.26) | copy-start | bytes 24580
  91.1 93.1 %reduce-scatter.3.cloned.1.call-start = ((), (), s32[]{:S(2)}) async-start(), calls=%async_computation.2 | async-start | bytes 1572864 | tf_op jit(solution)/shard_map/reduce_scatter | solution.py:120
  159.9 169.7 %all-gather.21.cloned.1.call-start = ((), (), s32[]{:S(2)}) async-start(), calls=%async_computation.9 | async-start | bytes 12255232 | tf_op jit(solution)/shard_map/all_gather | solution.py:137
  160.7 184.1 %all-gather.11.cloned.1.call-start = ((), (), s32[]{:S(2)}) async-start(), calls=%async_computation.3 | async-start | bytes 1572864 | tf_op jit(solution)/shard_map/all_gather | solution.py:138
  186.7 296.8 %all-gather.13.cloned.1.call-start = ((), (), s32[]{:S(2)}) async-start(), calls=%async_computation.4 | async-start | bytes 12255232 | tf_op jit(solution)/shard_map/all_gather | solution.py:134
  187.3 438.5 %all-gather.15.cloned.1.call-start = ((), (), s32[]{:S(2)}) async-start(), calls=%async_computation.5 | async-start | bytes 12255232 | tf_op jit(solution)/shard_map/all_gather | solution.py:135
  187.9 460.6 %reduce-scatter.5.cloned.1.call-start = ((), (), s32[]{:S(2)}) async-start(), calls=%async_computation.6 | async-start | bytes 1572864 | tf_op jit(solution)/shard_map/reduce_scatter | solution.py:143
  625.7 37.4 %copy-start.1 = (bf16[512,2048]{1,0:T(8,128)(2,1)S(1)}, bf16[512,2048]{1,0:T(8,128)(2,1)}, u32[]{:S(2)}) copy-start(bf16[512,2048]{1,0:T(8,128)(2,1)} %param.25) | copy-start | bytes 6291460
  641.7 19.1 %all-gather.17.cloned.1.call-start = ((), (), s32[]{:S(2)}) async-start(), calls=%async_computation.7 | async-start | bytes 1572864 | tf_op jit(solution)/shard_map/all_gather | solution.py:150
Sparse Core Ops, SparseCore 0:
  91.2 63.1 all-gather.18
  160.0 24.1 reduce-scatter.2
  187.0 142.6 all-gather.20
  331.0 7.1 all-gather.10
  340.9 142.5 all-gather.12
  486.1 139.5 all-gather.14
  641.8 6.5 reduce-scatter.4
  650.6 10.2 all-gather.16
